TPU v7x, 512 devices: a 4x2x32 block of a 4x8x32 slice. The times are simulated.
512 devices in a mesh: grp: 2 (over y), kv: 32 (over z), tp: 8 (over x, core).
Axes of the slice: x: 4, y: 2, z: 32, core: 2. Of those that a mesh axis runs over, the one named last changes fastest.
The devices are a block of a 4x8x32 slice.
Arguments:
- tokens: bfloat16 [256, 4096], P('grp', 'kv'), parts along dimension 0, may hold values from -40 to 40
- lengths: int32 [256], P(('grp', 'kv')), parts along dimension 0, may hold values from 1 to 6, 320 in all
- conv_state_x: bfloat16 [256, 3, 4096], P(('grp', 'kv'), None, 'tp'), parts along dimension 0, may hold values from -6 to 6
- conv_state_bc: bfloat16 [256, 3, 2, 1024], P(('grp', 'kv'), None, None, 'tp'), parts along dimension 0, may hold values from -6 to 6
- ssm_state: float32 [256, 64, 64, 128], P(('grp', 'kv'), 'tp'), parts along dimension 0, may hold values from -0.6 to 0.6
- norm_gain: bfloat16 [4096], P('kv'), may hold values from 0.099609375 to 1.8984375
- w_gate: bfloat16 [4096, 4096], P('kv', 'tp'), may hold values from -0.09375 to 0.09375
- w_value: bfloat16 [4096, 4096], P('kv', 'tp'), may hold values from -0.09375 to 0.09375
- w_key: bfloat16 [4096, 1024], P('kv', 'tp'), may hold values from -0.09375 to 0.09375
- w_query: bfloat16 [4096, 1024], P('kv', 'tp'), may hold values from -0.09375 to 0.09375
- w_step: bfloat16 [4096, 64], P('kv', 'tp'), may hold values from -0.09375 to 0.09375
- step_bias: float32 [64], P('tp'), may hold values from -2 to 0
- decay_log: float32 [64], P('tp'), may hold values from -2 to 1
- conv_x: bfloat16 [4, 4096], P(None, 'tp'), may hold values from -3 to 3
- conv_bc: bfloat16 [4, 2, 1024], P(None, None, 'tp'), may hold values from -3 to 3
- inner_gain: bfloat16 [4096], P('tp'), may hold values from 0.099609375 to 1.8984375
- w_out: bfloat16 [4096, 4096], P('tp', 'kv'), may hold values from -0.09375 to 0.09375
- mlp_gain: bfloat16 [4096], P('kv'), may hold values from 0.099609375 to 1.8984375
- w_up: bfloat16 [4096, 16384], P('kv', 'tp'), may hold values from -0.09375 to 0.09375
- w_down: bfloat16 [16384, 4096], P('tp', 'kv'), may hold values from -0.046875 to 0.046875
Outputs:
- layer_out: bfloat16 [256, 4096], P('grp', 'kv'), parts along dimension 0
- next_state: float32 [256, 64, 64, 128], P(('grp', 'kv'), 'tp'), parts along dimension 0
There are 2 independent parts, one for each index of `grp`. A program takes and returns all parts, laid end to end along the dimension named above; an argument that names none is the same for every part. Nothing has to cross between parts.
All inputs are finite; a program needn't handle non-finite values. No bound on the sum of `lengths` on one device may be relied on, other than what follows from the above.
Results may differ from a plain program's by a relative error of at most 0.008.
Values may be sent and summed in bfloat16 or wider, within the bound.
No kernel may reach another device: no remote copies, remote signals or barrier semaphores. Data moves between devices by JAX's collectives and lax.ppermute only.
A program may use at most 64 MiB of HBM per device.

v0:
```python
import jax
import jax.numpy as jnp
from jax import lax
from jax.sharding import PartitionSpec as P

D = 4096
HEAD_DIM = 64
STATE = 128
CONV_WIDTH = 4
INNER = 4096
epsilon = 1e-06


def in_blocks(shard, dim, size):
    before, after = (shard.shape[:dim], shard.shape[dim + 1 :])
    return jnp.moveaxis(shard.reshape(*before, size, -1, *after), dim, 0)


def summed_on_arrival(shard, axis, dim):
    parts = in_blocks(shard, dim, lax.axis_size(axis))
    arrived = lax.all_to_all(parts, axis, split_axis=0, concat_axis=0, tiled=True)
    return arrived.sum(axis=0)


def in_one_piece(arrays, axis, dim, along):
    columns = [a.reshape(*a.shape[:along], -1) for a in arrays]
    both = jnp.concatenate(columns, axis=along)
    filled, at, finished = (summed_on_arrival(both, axis, dim), 0, [])
    for a, column in zip(arrays, columns):
        slab = filled[..., at : at + column.shape[along]]
        finished.append(slab.reshape(*slab.shape[:along], *a.shape[along:]))
        at += column.shape[along]
    return tuple(finished)


def from_everyone(shard, axis):
    copies = jnp.broadcast_to(shard, (lax.axis_size(axis), *shard.shape))
    return lax.all_to_all(copies, axis, split_axis=0, concat_axis=0, tiled=True)


def over_copies(shard, axis):
    return from_everyone(shard, axis).sum(axis=0)


def laid_out(parts, dim):
    shape = list(parts.shape[1:])
    shape[dim] *= parts.shape[0]
    return jnp.moveaxis(parts, 0, dim).reshape(shape)


def gathered_copies(shard, axis, dim):
    parts = from_everyone(shard, axis)
    return laid_out(parts, dim)


def causal_conv(state_rows, newest, conv_weights):
    extended = jnp.concatenate([state_rows, newest[:, None]], axis=1)
    conv_sum = extended[:, 0] * conv_weights[0].astype(jnp.float32)
    for offset in range(1, conv_weights.shape[0]):
        conv_sum = conv_sum + extended[:, offset] * conv_weights[offset].astype(jnp.float32)
    return jax.nn.silu(conv_sum)


def product(left, right):
    return jnp.dot(left, right, preferred_element_type=jnp.float32)


def per_device(
    tokens,
    lengths,
    conv_state_x,
    conv_state_bc,
    ssm_state,
    norm_gain,
    w_gate,
    w_value,
    w_key,
    w_query,
    w_step,
    step_bias,
    decay_log,
    conv_x,
    conv_bc,
    inner_gain,
    w_out,
    mlp_gain,
    w_up,
    w_down,
):
    head_count = w_step.shape[1]
    group_count = w_key.shape[1] // STATE
    per_group = head_count // group_count
    widened = tokens.astype(jnp.float32)
    scaled = (widened * norm_gain.astype(jnp.float32)).astype(jnp.bfloat16)
    gate_raw, value_raw, key_raw, query_raw, step_raw, squares = in_one_piece(
        (
            product(scaled, w_gate),
            product(scaled, w_value),
            product(scaled, w_key),
            product(scaled, w_query),
            product(scaled, w_step),
            jnp.sum(widened * widened, axis=1),
        ),
        "kv",
        0,
        1,
    )
    seq_count = gate_raw.shape[0]
    inverse = lax.rsqrt(squares / D + epsilon)[:, None]
    row_live = (
        jnp.arange(CONV_WIDTH - 1, dtype=jnp.int32)[None, :] >= CONV_WIDTH - 1 - lengths[:, None]
    ).astype(jnp.float32)
    live_x = conv_state_x.astype(jnp.float32) * row_live[:, :, None]
    live_bc = conv_state_bc.astype(jnp.float32) * row_live[:, :, None, None]
    mixed_values = causal_conv(live_x, value_raw * inverse, conv_x).reshape(
        seq_count, head_count, HEAD_DIM
    )
    key_query = causal_conv(
        live_bc, jnp.stack([key_raw * inverse, query_raw * inverse], axis=1), conv_bc
    )
    key_heads = jnp.repeat(
        key_query[:, 0].reshape(seq_count, group_count, STATE), per_group, axis=1
    )
    query_heads = jnp.repeat(
        key_query[:, 1].reshape(seq_count, group_count, STATE), per_group, axis=1
    )
    step_size = jax.nn.softplus(step_raw * inverse + step_bias)
    rate_now = -jnp.exp(decay_log) * step_size
    next_state = (
        ssm_state * jnp.exp(rate_now)[:, :, None, None]
        + (step_size[:, :, None] * mixed_values)[:, :, :, None] * key_heads[:, :, None, :]
    )
    mixer_y = jnp.einsum(
        "bhpn,bhn->bhp", next_state, query_heads, precision=lax.Precision.HIGHEST
    ).reshape(seq_count, head_count * HEAD_DIM)
    gated_rows = mixer_y * jax.nn.silu(gate_raw * inverse)
    gated_low = (gated_rows * inner_gain.astype(jnp.float32)).astype(jnp.bfloat16)
    all_low, all_squares = (
        lax.all_gather(gated_low, "kv", axis=0, tiled=True),
        lax.all_gather(
            jnp.sum(gated_rows * gated_rows, axis=1).astype(jnp.bfloat16), "kv", axis=0, tiled=True
        ).astype(jnp.float32),
    )
    out_sum, gated_total = (
        over_copies(product(all_low, w_out), "tp"),
        over_copies(all_squares, "tp"),
    )
    residual = (widened + out_sum * lax.rsqrt(gated_total / INNER + epsilon)[:, None]).astype(
        jnp.bfloat16
    )
    residual_wide = residual.astype(jnp.float32)
    hidden_low = (residual_wide * mlp_gain.astype(jnp.float32)).astype(jnp.bfloat16)
    row_squares = jnp.sum(residual_wide * residual_wide, axis=1)
    up_share, square_share = in_one_piece((product(hidden_low, w_up), row_squares), "kv", 0, 1)
    share_active = jnp.square(
        jax.nn.relu(up_share * lax.rsqrt(square_share / D + epsilon)[:, None])
    ).astype(jnp.bfloat16)
    activation = gathered_copies(share_active, "kv", 0)
    down_sum = over_copies(product(activation, w_down), "tp")
    layer_out = (residual_wide + down_sum).astype(jnp.bfloat16)
    return (layer_out, next_state)


def solution(mesh):
    return jax.shard_map(
        per_device,
        mesh=mesh,
        in_specs=(
            P("grp", "kv"),
            P(("grp", "kv")),
            P(("grp", "kv"), None, "tp"),
            P(("grp", "kv"), None, None, "tp"),
            P(("grp", "kv"), "tp", None, None),
            P("kv"),
            P("kv", "tp"),
            P("kv", "tp"),
            P("kv", "tp"),
            P("kv", "tp"),
            P("kv", "tp"),
            P("tp"),
            P("tp"),
            P(None, "tp"),
            P(None, None, "tp"),
            P("tp"),
            P("tp", "kv"),
            P("kv"),
            P("kv", "tp"),
            P("tp", "kv"),
        ),
        out_specs=(P("grp", "kv"), P(("grp", "kv"), "tp", None, None)),
        check_vma=False,
    )
```

profile of v0, /device:TPU:33, one launch (start us, length us, event | category | flops | bytes accessed | tf_op | source)
XLA Modules:
  0.0 471.4 jit_solution(15149226765499633924)
XLA Ops:
  0.7 0.7 convert_element_type.73
  1.4 0.9 fusion.1
  2.5 0.9 fusion.16
  3.4 0.9 fusion.14
  4.3 0.9 fusion.12
  5.2 1.1 fusion.18
  6.8 1.2 concatenate.30
  8.0 46.4 %all-to-all-start = ((f32[32,4,1289]{2,1,0:T(4,128)}), f32[32,4,1289]{2,1,0:T(4,128)S(1)}, u32[]{:S(2)}, u32[]{:S(2)}) async-start(f32[32,4,1289]{2,1,0:T(4,128)} %concatenate.30), calls=%async_computation | async-start | bytes 1441792 | tf_op jit(solution)/shard_map/all_to_all | solution.py:21
  54.4 1.3 dynamic-slice
  56.6 79.0 %all-to-all-done = f32[32,4,1289]{2,1,0:T(4,128)S(1)} async-done(((f32[32,4,1289]{2,1,0:T(4,128)}), f32[32,4,1289]{2,1,0:T(4,128)S(1)}, u32[]{:S(2)}, u32[]{:S(2)}) %all-to-all-start) | async-done | bytes 660000 | tf_op jit(solution)/shard_map/all_to_all | solution.py:21
  136.3 0.4 multiply_add_fusion
  136.8 1.7 fusion.49
  139.1 39.4 %all-reduce = bf16[128]{0:T(256)(128)(2,1)S(1)} all-reduce(bf16[128]{0:T(256)(128)(2,1)S(1)} %dynamic-update-slice), channel_id=1, replica_groups=mesh['grp'=2,'kv'=32,'tp'=8] {'kv'}, use_global_device_ids=true, to_apply=%add | all-reduce | flops 128 | bytes 512
  178.5 0.6 broadcast_in_dim.9
  179.1 18.6 %all-to-all-start.2 = ((f32[8,1,128]{2,1,0:T(1,128)}), f32[8,1,128]{2,1,0:T(1,128)S(1)}, u32[]{:S(2)}, u32[]{:S(2)}) async-start(f32[8,1,128]{2,1,0:T(1,128)} %broadcast_in_dim.9), calls=%async_computation.2 | async-start | bytes 8192 | tf_op jit(solution)/shard_map/all_to_all | solution.py:38
  197.7 40.2 %all-gather = bf16[32,4,512]{2,1,0:T(4,128)(2,1)S(1)} all-gather(bf16[1,4,512]{2,1,0:T(4,128)(2,1)S(1)} %fusion.30), channel_id=1, replica_groups=mesh['grp'=2,'kv'=32,'tp'=8] {'kv'}, dimensions={0}, use_global_device_ids=true | all-gather | bytes 135168 | tf_op jit(solution)/shard_map/all_gather | solution.py:139
  238.2 0.8 broadcast_in_dim.8
  239.0 18.5 %all-to-all-start.1 = ((f32[8,128,128]{2,1,0:T(8,128)}), f32[8,128,128]{2,1,0:T(8,128)S(1)}, u32[]{:S(2)}, u32[]{:S(2)}) async-start(f32[8,128,128]{2,1,0:T(8,128)} %broadcast_in_dim.8), calls=%async_computation.1 | async-start | bytes 1048576 | tf_op jit(solution)/shard_map/all_to_all | solution.py:38
  257.6 9.3 %all-to-all-done.1 = f32[8,128,128]{2,1,0:T(8,128)S(1)} async-done(((f32[8,128,128]{2,1,0:T(8,128)}), f32[8,128,128]{2,1,0:T(8,128)S(1)}, u32[]{:S(2)}, u32[]{:S(2)}) %all-to-all-start.1) | async-done | bytes 524320 | tf_op jit(solution)/shard_map/all_to_all | solution.py:38
  267.7 0.3 concatenate.31
  268.2 120.2 %all_to_all.31 = f32[32,4,2049]{2,1,0:T(4,128)S(1)} all-to-all(f32[32,4,2049]{2,1,0:T(4,128)S(1)} %pad_maximum_fusion), channel_id=1, replica_groups=mesh['grp'=2,'kv'=32,'tp'=8] {'kv'}, dimensions={0} | all-to-all | bytes 2098176 | tf_op jit(solution)/shard_map/all_to_all | solution.py:21
  389.1 64.8 %all_to_all.32 = bf16[32,4,2048]{2,1,0:T(4,128)(2,1)S(1)} all-to-all(bf16[32,4,2048]{2,1,0:T(4,128)(2,1)S(1)} %broadcast_in_dim.10), channel_id=1, replica_groups=mesh['grp'=2,'kv'=32,'tp'=8] {'kv'}, dimensions={0} | all-to-all | bytes 1048576 | tf_op jit(solution)/shard_map/all_to_all | solution.py:38
  454.3 16.5 %all_to_all.33 = f32[8,128,128]{2,1,0:T(8,128)S(1)} all-to-all(f32[8,128,128]{2,1,0:T(8,128)S(1)} %broadcast_in_dim.11), channel_id=1, replica_groups=mesh['grp'=2,'kv'=32,'tp'=8] {'tp'}, dimensions={0} | all-to-all | bytes 1048576 | tf_op jit(solution)/shard_map/all_to_all | solution.py:38
  470.8 0.6 fusion.5
  (78 shorter events, 4.4 us)
Async XLA Ops:
  0.6 266.7 %copy-start = (bf16[128,2048]{1,0:T(8,128)(2,1)S(1)}, bf16[128,2048]{1,0:T(8,128)(2,1)}, u32[]{:S(2)}) copy-start(bf16[128,2048]{1,0:T(8,128)(2,1)} %param.38) | copy-start | bytes 1572868
  0.6 5.8 %copy-start.2 = (bf16[128,128]{1,0:T(8,128)(2,1)S(1)}, bf16[128,128]{1,0:T(8,128)(2,1)}, u32[]{:S(2)}) copy-start(bf16[128,128]{1,0:T(8,128)(2,1)} %param.20) | copy-start | bytes 98308
  0.7 5.8 %copy-start.6 = (bf16[128,512]{1,0:T(8,128)(2,1)S(1)}, bf16[128,512]{1,0:T(8,128)(2,1)}, u32[]{:S(2)}) copy-start(bf16[128,512]{1,0:T(8,128)(2,1)} %param.26) | copy-start | bytes 393220
  6.7 47.7 %copy-start.11 = (bf16[512]{0:T(512)(128)(2,1)S(1)}, bf16[512]{0:T(512)(128)(2,1)}, u32[]{:S(2)}) copy-start(bf16[512]{0:T(512)(128)(2,1)} %param.35) | copy-start | bytes 3076
  6.7 49.7 %copy-start.13 = (s32[4]{0:T(128)S(1)}, s32[4]{0:T(128)}, u32[]{:S(2)}) copy-start(s32[4]{0:T(128)} %param.21) | copy-start | bytes 52
  6.7 49.7 %copy-start.14 = (f32[8]{0:T(128)S(1)}, f32[8]{0:T(128)}, u32[]{:S(2)}) copy-start(f32[8]{0:T(128)} %param.32) | copy-start | bytes 100
  6.7 49.7 %copy-start.10 = (bf16[4,2,128]{2,1,0:T(2,128)(2,1)S(1)}, bf16[4,2,128]{2,1,0:T(2,128)(2,1)}, u32[]{:S(2)}) copy-start(bf16[4,2,128]{2,1,0:T(2,128)(2,1)} %param.34) | copy-start | bytes 6148
  6.7 49.7 %copy-start.7 = (bf16[4,512]{1,0:T(4,128)(2,1)S(1)}, bf16[4,512]{1,0:T(4,128)(2,1)}, u32[]{:S(2)}) copy-start(bf16[4,512]{1,0:T(4,128)(2,1)} %param.33) | copy-start | bytes 12292
  7.9 48.5 %copy-start.9 = (bf16[4,3,2,128]{3,2,1,0:T(2,128)(2,1)S(1)}, bf16[4,3,2,128]{3,2,1,0:T(2,128)(2,1)}, u32[]{:S(2)}) copy-start(bf16[4,3,2,128]{3,2,1,0:T(2,128)(2,1)} %param.23) | copy-start | bytes 18436
  7.9 48.6 %copy-start.8 = (bf16[4,3,512]{2,0,1:T(4,128)(2,1)S(1)}, bf16[4,3,512]{2,0,1:T(4,128)(2,1)}, u32[]{:S(2)}) copy-start(bf16[4,3,512]{2,0,1:T(4,128)(2,1)} %param.22) | copy-start | bytes 36868
  8.0 128.2 %copy-start.12 = (f32[8]{0:T(128)S(1)}, f32[8]{0:T(128)}, u32[]{:S(2)}) copy-start(f32[8]{0:T(128)} %param.31) | copy-start | bytes 100
  8.0 128.4 %copy-start.3 = (f32[4,8,64,128]{3,2,1,0:T(8,128)S(1)}, f32[4,8,64,128]{3,2,1,0:T(8,128)}, u32[]{:S(2)}) copy-start(f32[4,8,64,128]{3,2,1,0:T(8,128)} %param.24) | copy-start | bytes 3145732
  8.0 127.6 %all-to-all-start = ((f32[32,4,1289]{2,1,0:T(4,128)}), f32[32,4,1289]{2,1,0:T(4,128)S(1)}, u32[]{:S(2)}, u32[]{:S(2)}) async-start(f32[32,4,1289]{2,1,0:T(4,128)} %concatenate.30), calls=%async_computation | async-start | bytes 1441792 | tf_op jit(solution)/shard_map/all_to_all | solution.py:21
  136.8 102.2 %copy-start.1 = (f32[4,8,64,128]{3,2,1,0:T(8,128)}, f32[4,8,64,128]{3,2,1,0:T(8,128)S(1)}, u32[]{:S(2)}) copy-start(f32[4,8,64,128]{3,2,1,0:T(8,128)S(1)} %multiply_add_fusion) | copy-start | bytes 3145732
  136.8 101.2 %copy-start.5 = (bf16[512,128]{1,0:T(8,128)(2,1)S(1)}, bf16[512,128]{1,0:T(8,128)(2,1)}, u32[]{:S(2)}) copy-start(bf16[512,128]{1,0:T(8,128)(2,1)} %param.36) | copy-start | bytes 393220
  179.1 59.1 %all-to-all-start.2 = ((f32[8,1,128]{2,1,0:T(1,128)}), f32[8,1,128]{2,1,0:T(1,128)S(1)}, u32[]{:S(2)}, u32[]{:S(2)}) async-start(f32[8,1,128]{2,1,0:T(1,128)} %broadcast_in_dim.9), calls=%async_computation.2 | async-start | bytes 8192 | tf_op jit(solution)/shard_map/all_to_all | solution.py:38
  237.9 19.6 %copy-start.15 = (bf16[128]{0:T(256)(128)(2,1)S(1)}, bf16[128]{0:T(256)(128)(2,1)}, u32[]{:S(2)}) copy-start(bf16[128]{0:T(256)(128)(2,1)} %param.37) | copy-start | bytes 772
  239.0 27.9 %all-to-all-start.1 = ((f32[8,128,128]{2,1,0:T(8,128)}), f32[8,128,128]{2,1,0:T(8,128)S(1)}, u32[]{:S(2)}, u32[]{:S(2)}) async-start(f32[8,128,128]{2,1,0:T(8,128)} %broadcast_in_dim.8), calls=%async_computation.1 | async-start | bytes 1048576 | tf_op jit(solution)/shard_map/all_to_all | solution.py:38
  389.0 64.9 %copy-start.4 = (bf16[2048,128]{1,0:T(8,128)(2,1)S(1)}, bf16[2048,128]{1,0:T(8,128)(2,1)}, u32[]{:S(2)}) copy-start(bf16[2048,128]{1,0:T(8,128)(2,1)} %param.39) | copy-start | bytes 1572868
where the time goes:
time: 472 us; the launch traced here: 471 us
  blocking collectives  281 us (60%)
  waiting for transfers between devices  88.3 us (19%)
  starting transfers between devices  83.6 us (18%)
  matrix products  6.45 us (1%)
  local copies, waits for them, and re-layouts  5.78 us (1%)
    all_to_all x1, blocking collectives, summed_on_arrival(): lax.all_to_all(parts, axis, split_axis=0, concat_axis=0, tiled=True)  120 us
    all_to_all x2, blocking collectives, from_everyone(): return lax.all_to_all(copies, axis, split_axis=0, concat_axis=0, tiled=True)  81.3 us
    all_to_all x1, waiting for transfers between devices, summed_on_arrival(): lax.all_to_all(parts, axis, split_axis=0, concat_axis=0, tiled=True)  79 us
    all_to_all x1, starting transfers between devices, summed_on_arrival(): lax.all_to_all(parts, axis, split_axis=0, concat_axis=0, tiled=True)  46.4 us
    all_gather x1, blocking collectives, per_device(): lax.all_gather(gated_low, 'kv', axis=0, tiled=True)  40.2 us
    unnamed x1, blocking collectives  39.4 us
    all_to_all x2, starting transfers between devices, from_everyone(): return lax.all_to_all(copies, axis, split_axis=0, concat_axis=0, tiled=True)  37.2 us
  transfers between devices with their start and end apart: 3, of which 2 were waited for; matrix products, arithmetic and copies ran while one was open for 0% of the time, Pallas kernels for 0%

commit v1 on v0

--- a/solution.py
+++ b/solution.py
@@ -9,6 +9,11 @@
 CONV_WIDTH = 4
 INNER = 4096
 epsilon = 1e-06
+
+
+def gather_by_exchange(x, axis, dim):
+    copies = jnp.concatenate([x] * lax.axis_size(axis), axis=dim)
+    return lax.all_to_all(copies, axis, dim, dim, tiled=True)
 
 
 def in_blocks(shard, dim, size):
@@ -136,7 +141,7 @@
     gated_rows = mixer_y * jax.nn.silu(gate_raw * inverse)
     gated_low = (gated_rows * inner_gain.astype(jnp.float32)).astype(jnp.bfloat16)
     all_low, all_squares = (
-        lax.all_gather(gated_low, "kv", axis=0, tiled=True),
+        gather_by_exchange(gated_low, "kv", 0),
         lax.all_gather(
             jnp.sum(gated_rows * gated_rows, axis=1).astype(jnp.bfloat16), "kv", axis=0, tiled=True
         ).astype(jnp.float32),

time: 472 us -> 452 us (0.958)
  blocking collectives: 281 us -> 263 us
  starting transfers between devices: 83.6 us -> 73.2 us
  waiting for transfers between devices: 88.3 us -> 94.5 us
    all_gather x1 -> x0, blocking collectives: 40.2 us -> none  [per_device(): lax.all_gather(gated_low, 'kv', axis=0, tiled=True)]
    all_to_all x2, starting transfers between devices: 37.2 us -> 22 us  [from_everyone(): return lax.all_to_all(copies, axis, split_axis=0, concat_axis=0, tiled=True)]
    all_to_all x1, blocking collectives: 120 us -> 133 us  [summed_on_arrival(): lax.all_to_all(parts, axis, split_axis=0, concat_axis=0, tiled=True)]
    unnamed x1, blocking collectives: 39.4 us -> 48.8 us
    all_to_all x0 -> x1, starting transfers between devices: none -> 4.77 us  [gather_by_exchange(): return lax.all_to_all(copies, axis, dim, dim, tiled=True)]
  transfers between devices with their start and end apart: 3 -> 4, of which waited for: 2 -> 3; matrix products, arithmetic and copies ran while one was open for 0% -> 0% of each run, Pallas kernels for 0% -> 0%
where the time goes in v1:
time: 452 us; the launch traced here: 451 us
  blocking collectives  263 us (58%)
  waiting for transfers between devices  94.5 us (21%)
  starting transfers between devices  73.2 us (16%)
  local copies, waits for them, and re-layouts  7.02 us (2%)
  matrix products  6.45 us (1%)
  other arithmetic  4.55 us (1%)
    all_to_all x1, blocking collectives, summed_on_arrival(): lax.all_to_all(parts, axis, split_axis=0, concat_axis=0, tiled=True)  133 us
    all_to_all x2, blocking collectives, from_everyone(): return lax.all_to_all(copies, axis, split_axis=0, concat_axis=0, tiled=True)  81.3 us
    all_to_all x1, waiting for transfers between devices, summed_on_arrival(): lax.all_to_all(parts, axis, split_axis=0, concat_axis=0, tiled=True)  80.8 us
    unnamed x1, blocking collectives  48.8 us
    all_to_all x1, starting transfers between devices, summed_on_arrival(): lax.all_to_all(parts, axis, split_axis=0, concat_axis=0, tiled=True)  46.4 us
    all_to_all x2, starting transfers between devices, from_everyone(): return lax.all_to_all(copies, axis, split_axis=0, concat_axis=0, tiled=True)  22 us
    all_to_all x2, waiting for transfers between devices, from_everyone(): return lax.all_to_all(copies, axis, split_axis=0, concat_axis=0, tiled=True)  13.7 us
  transfers between devices with their start and end apart: 4, of which 3 were waited for; matrix products, arithmetic and copies ran while one was open for 0% of the time, Pallas kernels for 0%

profile of v1, /device:TPU:33, one launch (start us, length us, event | category | flops | bytes accessed | tf_op | source)
XLA Modules:
  0.0 450.8 jit_solution(11315961585116401028)
XLA Ops:
  0.7 0.7 convert_element_type.73
  1.4 0.9 fusion.1
  2.5 0.9 fusion.16
  3.4 0.9 fusion.14
  4.3 0.9 fusion.12
  5.2 1.1 fusion.18
  6.8 1.2 concatenate.33
  8.0 46.4 %all-to-all-start = ((f32[32,4,1289]{2,1,0:T(4,128)}), f32[32,4,1289]{2,1,0:T(4,128)S(1)}, u32[]{:S(2)}, u32[]{:S(2)}) async-start(f32[32,4,1289]{2,1,0:T(4,128)} %concatenate.33), calls=%async_computation | async-start | bytes 1441792 | tf_op jit(solution)/shard_map/all_to_all | solution.py:26
  54.8 80.8 %all-to-all-done = f32[32,4,1289]{2,1,0:T(4,128)S(1)} async-done(((f32[32,4,1289]{2,1,0:T(4,128)}), f32[32,4,1289]{2,1,0:T(4,128)S(1)}, u32[]{:S(2)}, u32[]{:S(2)}) %all-to-all-start) | async-done | bytes 660000 | tf_op jit(solution)/shard_map/all_to_all | solution.py:26
  136.8 1.7 fusion.47
  139.3 0.7 all_to_all.28
  140.0 4.8 %all-to-all-start.1 = ((bf16[32,4,512]{2,1,0:T(4,128)(2,1)}), bf16[32,4,512]{2,1,0:T(4,128)(2,1)S(1)}, u32[]{:S(2)}, u32[]{:S(2)}) async-start(bf16[32,4,512]{2,1,0:T(4,128)(2,1)} %all_to_all.28), calls=%async_computation.1 | async-start | bytes 262144 | tf_op jit(solution)/shard_map/all_to_all | solution.py:16
  144.8 1.3 dynamic-slice
  146.9 48.8 %all-reduce = bf16[128]{0:T(256)(128)(2,1)S(1)} all-reduce(bf16[128]{0:T(256)(128)(2,1)S(1)} %dynamic-update-slice), channel_id=1, replica_groups=mesh['grp'=2,'kv'=32,'tp'=8] {'kv'}, use_global_device_ids=true, to_apply=%add | all-reduce | flops 128 | bytes 512
  195.8 0.6 broadcast_in_dim.9
  196.3 17.9 %all-to-all-start.3 = ((f32[8,1,128]{2,1,0:T(1,128)}), f32[8,1,128]{2,1,0:T(1,128)S(1)}, u32[]{:S(2)}, u32[]{:S(2)}) async-start(f32[8,1,128]{2,1,0:T(1,128)} %broadcast_in_dim.9), calls=%async_computation.3 | async-start | bytes 8192 | tf_op jit(solution)/shard_map/all_to_all | solution.py:43
  214.5 4.3 all-to-all-done.3
  218.8 0.8 broadcast_in_dim.8
  219.6 4.1 all-to-all-start.2
  223.7 9.4 %all-to-all-done.2 = f32[8,128,128]{2,1,0:T(8,128)S(1)} async-done(((f32[8,128,128]{2,1,0:T(8,128)}), f32[8,128,128]{2,1,0:T(8,128)S(1)}, u32[]{:S(2)}, u32[]{:S(2)}) %all-to-all-start.2) | async-done | bytes 524320 | tf_op jit(solution)/shard_map/all_to_all | solution.py:43
  234.5 133.3 %all_to_all.43 = f32[32,4,2049]{2,1,0:T(4,128)S(1)} all-to-all(f32[32,4,2049]{2,1,0:T(4,128)S(1)} %pad_maximum_fusion), channel_id=1, replica_groups=mesh['grp'=2,'kv'=32,'tp'=8] {'kv'}, dimensions={0} | all-to-all | bytes 2098176 | tf_op jit(solution)/shard_map/all_to_all | solution.py:26
  368.4 64.8 %all_to_all.44 = bf16[32,4,2048]{2,1,0:T(4,128)(2,1)S(1)} all-to-all(bf16[32,4,2048]{2,1,0:T(4,128)(2,1)S(1)} %broadcast_in_dim.10), channel_id=1, replica_groups=mesh['grp'=2,'kv'=32,'tp'=8] {'kv'}, dimensions={0} | all-to-all | bytes 1048576 | tf_op jit(solution)/shard_map/all_to_all | solution.py:43
  433.6 16.5 %all_to_all.45 = f32[8,128,128]{2,1,0:T(8,128)S(1)} all-to-all(f32[8,128,128]{2,1,0:T(8,128)S(1)} %broadcast_in_dim.11), channel_id=1, replica_groups=mesh['grp'=2,'kv'=32,'tp'=8] {'tp'}, dimensions={0} | all-to-all | bytes 1048576 | tf_op jit(solution)/shard_map/all_to_all | solution.py:43
  450.1 0.6 fusion.5
  (82 shorter events, 5.7 us)
Async XLA Ops:
  0.6 233.0 %copy-start = (bf16[128,2048]{1,0:T(8,128)(2,1)S(1)}, bf16[128,2048]{1,0:T(8,128)(2,1)}, u32[]{:S(2)}) copy-start(bf16[128,2048]{1,0:T(8,128)(2,1)} %param.38) | copy-start | bytes 1572868
  0.6 5.8 %copy-start.2 = (bf16[128,128]{1,0:T(8,128)(2,1)S(1)}, bf16[128,128]{1,0:T(8,128)(2,1)}, u32[]{:S(2)}) copy-start(bf16[128,128]{1,0:T(8,128)(2,1)} %param.20) | copy-start | bytes 98308
  0.7 5.8 %copy-start.6 = (bf16[128,512]{1,0:T(8,128)(2,1)S(1)}, bf16[128,512]{1,0:T(8,128)(2,1)}, u32[]{:S(2)}) copy-start(bf16[128,512]{1,0:T(8,128)(2,1)} %param.26) | copy-start | bytes 393220
  6.7 47.7 %copy-start.13 = (s32[4]{0:T(128)S(1)}, s32[4]{0:T(128)}, u32[]{:S(2)}) copy-start(s32[4]{0:T(128)} %param.21) | copy-start | bytes 52
  6.7 47.8 %copy-start.11 = (bf16[512]{0:T(512)(128)(2,1)S(1)}, bf16[512]{0:T(512)(128)(2,1)}, u32[]{:S(2)}) copy-start(bf16[512]{0:T(512)(128)(2,1)} %param.35) | copy-start | bytes 3076
  6.7 47.8 %copy-start.14 = (f32[8]{0:T(128)S(1)}, f32[8]{0:T(128)}, u32[]{:S(2)}) copy-start(f32[8]{0:T(128)} %param.32) | copy-start | bytes 100
  6.7 47.8 %copy-start.10 = (bf16[4,2,128]{2,1,0:T(2,128)(2,1)S(1)}, bf16[4,2,128]{2,1,0:T(2,128)(2,1)}, u32[]{:S(2)}) copy-start(bf16[4,2,128]{2,1,0:T(2,128)(2,1)} %param.34) | copy-start | bytes 6148
  6.7 47.8 %copy-start.7 = (bf16[4,512]{1,0:T(4,128)(2,1)S(1)}, bf16[4,512]{1,0:T(4,128)(2,1)}, u32[]{:S(2)}) copy-start(bf16[4,512]{1,0:T(4,128)(2,1)} %param.33) | copy-start | bytes 12292
  7.9 46.7 %copy-start.9 = (bf16[4,3,2,128]{3,2,1,0:T(2,128)(2,1)S(1)}, bf16[4,3,2,128]{3,2,1,0:T(2,128)(2,1)}, u32[]{:S(2)}) copy-start(bf16[4,3,2,128]{3,2,1,0:T(2,128)(2,1)} %param.23) | copy-start | bytes 18436
  7.9 46.7 %copy-start.8 = (bf16[4,3,512]{2,0,1:T(4,128)(2,1)S(1)}, bf16[4,3,512]{2,0,1:T(4,128)(2,1)}, u32[]{:S(2)}) copy-start(bf16[4,3,512]{2,0,1:T(4,128)(2,1)} %param.22) | copy-start | bytes 36868
  8.0 128.2 %copy-start.12 = (f32[8]{0:T(128)S(1)}, f32[8]{0:T(128)}, u32[]{:S(2)}) copy-start(f32[8]{0:T(128)} %param.31) | copy-start | bytes 100
  8.0 128.4 %copy-start.3 = (f32[4,8,64,128]{3,2,1,0:T(8,128)S(1)}, f32[4,8,64,128]{3,2,1,0:T(8,128)}, u32[]{:S(2)}) copy-start(f32[4,8,64,128]{3,2,1,0:T(8,128)} %param.24) | copy-start | bytes 3145732
  8.0 127.6 %all-to-all-start = ((f32[32,4,1289]{2,1,0:T(4,128)}), f32[32,4,1289]{2,1,0:T(4,128)S(1)}, u32[]{:S(2)}, u32[]{:S(2)}) async-start(f32[32,4,1289]{2,1,0:T(4,128)} %concatenate.33), calls=%async_computation | async-start | bytes 1441792 | tf_op jit(solution)/shard_map/all_to_all | solution.py:26
  136.8 77.5 %copy-start.1 = (f32[4,8,64,128]{3,2,1,0:T(8,128)}, f32[4,8,64,128]{3,2,1,0:T(8,128)S(1)}, u32[]{:S(2)}) copy-start(f32[4,8,64,128]{3,2,1,0:T(8,128)S(1)} %multiply_add_fusion) | copy-start | bytes 3145732
  136.8 77.5 %copy-start.5 = (bf16[512,128]{1,0:T(8,128)(2,1)S(1)}, bf16[512,128]{1,0:T(8,128)(2,1)}, u32[]{:S(2)}) copy-start(bf16[512,128]{1,0:T(8,128)(2,1)} %param.36) | copy-start | bytes 393220
  140.0 55.8 %all-to-all-start.1 = ((bf16[32,4,512]{2,1,0:T(4,128)(2,1)}), bf16[32,4,512]{2,1,0:T(4,128)(2,1)S(1)}, u32[]{:S(2)}, u32[]{:S(2)}) async-start(bf16[32,4,512]{2,1,0:T(4,128)(2,1)} %all_to_all.28), calls=%async_computation.1 | async-start | bytes 262144 | tf_op jit(solution)/shard_map/all_to_all | solution.py:16
  196.3 22.4 %all-to-all-start.3 = ((f32[8,1,128]{2,1,0:T(1,128)}), f32[8,1,128]{2,1,0:T(1,128)S(1)}, u32[]{:S(2)}, u32[]{:S(2)}) async-start(f32[8,1,128]{2,1,0:T(1,128)} %broadcast_in_dim.9), calls=%async_computation.3 | async-start | bytes 8192 | tf_op jit(solution)/shard_map/all_to_all | solution.py:43
  214.2 9.5 %copy-start.15 = (bf16[128]{0:T(256)(128)(2,1)S(1)}, bf16[128]{0:T(256)(128)(2,1)}, u32[]{:S(2)}) copy-start(bf16[128]{0:T(256)(128)(2,1)} %param.37) | copy-start | bytes 772
  219.6 13.5 %all-to-all-start.2 = ((f32[8,128,128]{2,1,0:T(8,128)}), f32[8,128,128]{2,1,0:T(8,128)S(1)}, u32[]{:S(2)}, u32[]{:S(2)}) async-start(f32[8,128,128]{2,1,0:T(8,128)} %broadcast_in_dim.8), calls=%async_computation.2 | async-start | bytes 1048576 | tf_op jit(solution)/shard_map/all_to_all | solution.py:43
  368.3 65.0 %copy-start.4 = (bf16[2048,128]{1,0:T(8,128)(2,1)S(1)}, bf16[2048,128]{1,0:T(8,128)(2,1)}, u32[]{:S(2)}) copy-start(bf16[2048,128]{1,0:T(8,128)(2,1)} %param.39) | copy-start | bytes 1572868
